TPU v7x, 512 devices: a 4x2x32 block of a 4x8x32 slice. The times are simulated.
512 devices in a mesh: grp: 2 (over y), fs: 32 (over z), tp: 8 (over x, core).
Axes of the slice: x: 4, y: 2, z: 32, core: 2. Of those that a mesh axis runs over, the one named last changes fastest.
The devices are a block of a 4x8x32 slice.
Arguments:
- stream: bfloat16 [64, 128, 2048], P(('grp', 'fs')), parts along dimension 0, may hold values from -6 to 6
- in_gain: float32 [2048], replicated, may hold values from 0.2 to 5
- value_weight: bfloat16 [2048, 1024], P('fs', 'tp'), may hold values from -0.125 to 0.125
- gate_weight: bfloat16 [2048, 1024], P('fs', 'tp'), may hold values from -0.125 to 0.125
- conv_kernel: bfloat16 [31, 1024], P(None, 'tp'), may hold values from -3.6 to 3.6
- conv_gain: float32 [1024], P('tp'), may hold values from 0.1 to 1.9
- conv_shift: float32 [1024], P('tp'), may hold values from -3 to 3
- out_weight: bfloat16 [1024, 2048], P('tp', 'fs'), may hold values from -0.1875 to 0.1875
- norm_gain: float32 [2048], replicated, may hold values from 0.2 to 5
- up_weight: bfloat16 [2048, 8192], P('fs', 'tp'), may hold values from -0.125 to 0.125
- down_weight: bfloat16 [8192, 2048], P('tp', 'fs'), may hold values from -0.0625 to 0.0625
- out_gain: float32 [2048], P('tp'), may hold values from 0.1 to 1.9
Outputs:
- result: bfloat16 [64, 128, 2048], P(('grp', 'fs'), None, 'tp'), parts along dimension 0
There are 2 independent parts, one for each index of `grp`. A program takes and returns all parts, laid end to end along the dimension named above; an argument that names none is the same for every part. Nothing has to cross between parts.
All inputs are finite; a program needn't handle non-finite values.
Results may differ from a plain program's by a relative error of at most 0.02.
Values may be sent and summed in bfloat16 or wider, within the bound.
No kernel may reach another device: no remote copies, remote signals or barrier semaphores. Data moves between devices by JAX's collectives and lax.ppermute only.
A program may use at most 64 MiB of HBM per device.

v0:
```python
import jax
import jax.numpy as jnp
from jax import lax
from jax.sharding import PartitionSpec as P

KW = 31
norm_epsilon = 1e-05
residual_scale = 2.0**0.25
feature_scale = 2.0**7


def to_half(x, scale):
    return (x.astype(jnp.float32) * scale).astype(jnp.float16)


def from_half(x, scale):
    return (x.astype(jnp.float32) * (1 / scale)).astype(jnp.bfloat16)


def gather_fs(x):
    return lax.all_gather(x, "fs", axis=0, tiled=True)


def in_order(is_even, mine, theirs):
    return (jnp.where(is_even, mine, theirs), jnp.where(is_even, theirs, mine))


def norm_rows(values, gain_vector):
    row_mean = jnp.mean(values, axis=-1, keepdims=True)
    row_var = jnp.mean(jnp.square(values - row_mean), axis=-1, keepdims=True)
    return (values - row_mean) * lax.rsqrt(row_var + norm_epsilon) * gain_vector


def contract(left, turned):
    return lax.dot_general(
        left, turned, (((1,), (1,)), ((), ())), preferred_element_type=jnp.float32
    )


def swap_blocks(x):
    return lax.all_to_all(x, "tp", 0, 0, tiled=True)


def summed(tiles):
    return jnp.sum(tiles.astype(jnp.float32), axis=0).astype(jnp.bfloat16)


def shards(
    stream,
    in_gain,
    value_weight,
    gate_weight,
    conv_kernel,
    conv_gain,
    conv_shift,
    out_weight,
    norm_gain,
    up_weight,
    down_weight,
    out_gain,
):
    seq_count, seq_length, model_width = stream.shape
    token_count = seq_count * seq_length
    tp_count = lax.axis_size("tp")
    group_count = lax.axis_size("grp")
    slice_width = model_width // tp_count
    own_tokens = token_count // tp_count
    tp_index = lax.axis_index("tp")
    channels = value_weight.shape[1]
    sharing = 2 if group_count % 2 == 0 else 1
    partner = [(g, g ^ 1) for g in range(group_count)]
    is_even = lax.axis_index("grp") % 2 == 0
    teams = [
        [g * tp_count + t for t in range(tp_count) for g in range(first, first + sharing)]
        for first in range(0, group_count, sharing)
    ]
    share = up_weight.shape[1] // sharing
    up_shard, down_shard = (up_weight, down_weight.T)
    if sharing == 2:
        up_shard = jnp.where(is_even, up_shard[:, :share], up_shard[:, share:])
        down_shard = jnp.where(is_even, down_shard[:, :share], down_shard[:, share:])
    feed = gather_fs(jnp.concatenate([up_shard, down_shard], axis=1))
    up_whole, down_turned = (feed[:, :share], feed[:, share:])
    rows = value_weight.shape[0]
    half = rows // 2
    out_shard = out_weight.T
    even_part = jnp.concatenate([value_weight, out_shard[:half]], axis=0)
    odd_part = jnp.concatenate([gate_weight, out_shard[half:]], axis=0)
    if sharing == 2:
        mine = gather_fs(jnp.where(is_even, even_part, odd_part))
        theirs = lax.ppermute(mine, "grp", partner)
        even_whole, odd_whole = in_order(is_even, mine, theirs)
    else:
        even_whole, odd_whole = (gather_fs(even_part), gather_fs(odd_part))
    even_whole = even_whole.reshape(-1, rows + half, channels)
    odd_whole = odd_whole.reshape(-1, rows + half, channels)
    value_whole = even_whole[:, :rows].reshape(-1, channels)
    gate_whole = odd_whole[:, :rows].reshape(-1, channels)
    out_turned = jnp.concatenate([even_whole[:, rows:], odd_whole[:, rows:]], axis=1).reshape(
        -1, channels
    )
    normed = norm_rows(
        stream.reshape(token_count, model_width).astype(jnp.float32), in_gain
    ).astype(jnp.bfloat16)
    values = jnp.dot(normed, value_whole, preferred_element_type=jnp.float32)
    gating = jnp.dot(normed, gate_whole, preferred_element_type=jnp.float32)
    gated = (values * jax.nn.sigmoid(gating)).astype(jnp.bfloat16)
    convolved = lax.conv_general_dilated(
        gated.reshape(seq_count, seq_length, channels),
        conv_kernel[:, None, :],
        window_strides=(1,),
        padding=[(KW - 1, 0)],
        dimension_numbers=("NWC", "WIO", "NWC"),
        feature_group_count=channels,
        preferred_element_type=jnp.float32,
    ).reshape(token_count, channels)
    told = jnp.concatenate(
        [jnp.sum(convolved, axis=1), jnp.sum(convolved * convolved, axis=1), out_gain]
    )
    normed_own = lax.dynamic_slice_in_dim(normed, tp_index * own_tokens, own_tokens, 0)
    told, out_turned, normed_own, norm_gain = lax.optimization_barrier(
        (told, out_turned, normed_own, norm_gain)
    )
    heard = swap_blocks(jnp.broadcast_to(told[None], (tp_count, *told.shape)))
    sums = jnp.sum(heard[:, : 2 * token_count], axis=0).reshape(2, token_count)
    whole_gain = heard[:, 2 * token_count :].reshape(model_width)
    row_mean = sums[0] / (channels * tp_count)
    row_var = sums[1] / (channels * tp_count) - row_mean * row_mean
    activated = jax.nn.silu(
        (convolved - row_mean[:, None]) * lax.rsqrt(row_var + norm_epsilon)[:, None] * conv_gain
        + conv_shift
    ).astype(jnp.bfloat16)
    mixed_terms = contract(activated, out_turned).astype(jnp.bfloat16)
    mixed_terms, whole_gain = lax.optimization_barrier((mixed_terms, whole_gain))
    mixed = summed(swap_blocks(mixed_terms.reshape(tp_count, own_tokens, model_width)))
    settled_own = norm_rows(
        residual_scale * normed_own.astype(jnp.float32) + mixed.astype(jnp.float32), norm_gain
    ).astype(jnp.bfloat16)
    if sharing == 2:
        their_settled = lax.ppermute(settled_own, "grp", partner)
        pair_settled = jnp.stack(in_order(is_even, settled_own, their_settled))
    else:
        pair_settled = settled_own[None]
    settled = from_half(
        lax.all_gather(to_half(pair_settled, feature_scale), "tp", axis=0, tiled=True),
        feature_scale,
    ).reshape(sharing * token_count, model_width)
    hidden = jnp.square(
        jax.nn.relu(jnp.dot(settled, up_whole, preferred_element_type=jnp.float32))
    ).astype(jnp.bfloat16)
    hidden = lax.optimization_barrier(hidden)
    fed_terms = contract(hidden, down_turned).astype(jnp.bfloat16)
    fed = summed(
        lax.all_to_all(
            fed_terms.reshape(sharing * tp_count, own_tokens, model_width),
            ("grp", "tp"),
            0,
            0,
            tiled=True,
            axis_index_groups=teams,
        )
    )
    result_own = norm_rows(
        residual_scale * settled_own.astype(jnp.float32) + fed.astype(jnp.float32), whole_gain
    ).astype(jnp.bfloat16)
    pieces = jnp.moveaxis(result_own.reshape(own_tokens, tp_count, slice_width), 1, 0)
    return swap_blocks(pieces).reshape(seq_count, seq_length, slice_width)


def solution(mesh):
    in_specs = (
        P(("grp", "fs"), None, None),
        P(),
        P("fs", "tp"),
        P("fs", "tp"),
        P(None, "tp"),
        P("tp"),
        P("tp"),
        P("tp", "fs"),
        P(),
        P("fs", "tp"),
        P("tp", "fs"),
        P("tp"),
    )
    out_specs = P(("grp", "fs"), None, "tp")
    return jax.shard_map(shards, mesh=mesh, in_specs=in_specs, out_specs=out_specs, check_vma=False)
```

profile of v0, /device:TPU:33, one launch (start us, length us, event | category | flops | bytes accessed | tf_op | source)
XLA Modules:
  0.0 217.8 jit_solution(2617139166442563405)
XLA Ops:
  6.5 0.0 copy-start
  6.6 0.0 copy-start.1
  6.6 0.0 copy-start.2
  6.6 0.0 all-gather.3.cloned.1.call-start
  6.6 1.0 slice_select_fusion
  7.6 0.7 pad_maximum_fusion.1
  8.2 0.1 all-gather.3.cloned.1.call-update
  8.3 0.7 fusion.37
  9.0 0.7 maximum_select_fusion
  9.8 89.2 %all_gather.9 = bf16[3072,128]{1,0:T(8,128)(2,1)S(1)} all-gather(bf16[96,128]{1,0:T(8,128)(2,1)S(1)} %maximum_select_fusion), channel_id=1, replica_groups=mesh['grp'=2,'fs'=32,'tp'=8] {'fs'}, dimensions={0}, use_global_device_ids=true | all-gather | bytes 811008 | tf_op jit(solution)/shard_map/all_gather | solution.py:21
  98.9 6.8 %collective-permute-start = (bf16[3072,128]{1,0:T(8,128)(2,1)S(1)}, bf16[3072,128]{1,0:T(8,128)(2,1)S(1)}, u32[]{:S(2)}, u32[]{:S(2)}) collective-permute-start(bf16[3072,128]{1,0:T(8,128)(2,1)S(1)} %all_gather.9), channel_id=1, source_target_pairs={{0,256},{256,0},{1,257},{257,1},{2,258},{258,2},{3,259},{259,3},{4... | collective-permute-start | bytes 2359304 | tf_op jit(solution)/shard_map/ppermute | solution.py:91
  105.8 0.0 copy-done.1
  105.8 0.2 convert_reduce_fusion
  106.0 0.3 fusion.20
  106.3 0.1 dynamic-slice
  106.3 0.0 copy-done.2
  106.3 0.1 fusion.23
  106.4 9.1 %collective-permute-done = bf16[3072,128]{1,0:T(8,128)(2,1)S(1)} collective-permute-done((bf16[3072,128]{1,0:T(8,128)(2,1)S(1)}, bf16[3072,128]{1,0:T(8,128)(2,1)S(1)}, u32[]{:S(2)}, u32[]{:S(2)}) %collective-permute-start) | collective-permute-done | bytes 786464 | tf_op jit(solution)/shard_map/ppermute | solution.py:91
  115.6 0.1 broadcast_select_fusion.1
  115.7 0.1 slice.69
  115.8 0.1 slice.68
  115.9 0.0 copy-start.4
  115.9 0.4 fusion.14
  116.3 0.0 copy-start.5
  116.3 0.0 copy-start.6
  116.3 0.4 fusion.16
  116.7 0.0 copy-done
  116.7 1.1 fusion.38
  117.8 0.1 multiply_reduce_fusion.3
  117.9 0.0 copy-done.4
  117.9 0.0 copy-start.3
  117.9 0.1 pad_maximum_fusion
  118.0 20.6 %all_to_all.24 = f32[8,1,512]{2,1,0:T(1,128)S(1)} all-to-all(f32[8,1,512]{2,1,0:T(1,128)S(1)} %broadcast_in_dim.5), channel_id=1, replica_groups=mesh['grp'=2,'fs'=32,'tp'=8] {'tp'}, dimensions={0} | all-to-all | bytes 32768 | tf_op jit(solution)/shard_map/all_to_all | solution.py:41
  138.6 0.0 copy-done.5
  138.6 0.0 copy-done.6
  138.6 0.4 convolution_convert_fusion.1
  139.0 12.5 %all_to_all.25 = bf16[8,16,2048]{2,1,0:T(8,128)(2,1)S(1)} all-to-all(bf16[8,16,2048]{2,1,0:T(8,128)(2,1)S(1)} %bitcast.53), channel_id=1, replica_groups=mesh['grp'=2,'fs'=32,'tp'=8] {'tp'}, dimensions={0} | all-to-all | bytes 1048576 | tf_op jit(solution)/shard_map/all_to_all | solution.py:41
  151.5 0.1 reduce_sum.110
  151.6 0.1 fusion.24
  151.7 0.2 multiply_reduce_fusion.2
  152.0 0.0 copy-done.3
  152.0 0.1 multiply_convert_fusion.3
  152.1 3.7 %collective-permute-start.1 = (bf16[16,2048]{1,0:T(8,128)(2,1)S(1)}, bf16[16,2048]{1,0:T(8,128)(2,1)S(1)}, u32[]{:S(2)}, u32[]{:S(2)}) collective-permute-start(bf16[16,2048]{1,0:T(8,128)(2,1)S(1)} %multiply_convert_fusion.3), channel_id=1, source_target_pairs={{0,256},{256,0},{1,257},{257,1},{2,258},{258,2},{3,259},{259,3},{4... | collective-permute-start | bytes 196616 | tf_op jit(solution)/shard_map/ppermute | solution.py:140
  155.8 2.0 collective-permute-done.1
  157.9 15.3 %all-gather.4 = f16[16,16,2048]{2,1,0:T(8,128)(2,1)S(1)} all-gather(f16[2,16,2048]{2,1,0:T(8,128)(2,1)S(1)} %multiply_convert_fusion.1), channel_id=1, replica_groups=mesh['grp'=2,'fs'=32,'tp'=8] {'tp'}, dimensions={0}, use_global_device_ids=true | all-gather | bytes 1179648 | tf_op jit(solution)/shard_map/all_gather | solution.py:145
  173.1 0.2 multiply_convert_fusion
  173.3 0.0 all-gather.3.cloned.1.call-done
  173.4 0.0 copy-start.7
  173.4 2.4 %fusion.9 = bf16[256,512]{1,0:T(8,128)(2,1)S(1)} fusion(bf16[256,2048]{1,0:T(8,128)(2,1)S(1)} %bitcast.54, bf16[2048,1024]{1,0:T(8,128)(2,1)} %all-gather.3.cloned.1.call-done), kind=kOutput, calls=%fused_computation.11 | convolution fusion | flops 537264128 | bytes 3407872 | tf_op jit(solution)/shard_map/dot_general | solution.py:149
  175.8 0.4 copy-done.7
  176.2 0.7 convolution_convert_fusion
  176.9 24.6 %all_to_all.26 = bf16[16,16,2048]{2,1,0:T(8,128)(2,1)S(1)} all-to-all(bf16[16,16,2048]{2,1,0:T(8,128)(2,1)S(1)} %bitcast.55), channel_id=1, replica_groups={{0,256,1,257,2,258,3,259,4,260,5,261,6,262,7,263},{8,264,9,265,10,266,1..., dimensions={0} | all-to-all | bytes 2097152 | tf_op jit(solution)/shard_map/all_to_all | solution.py:154
  201.5 0.1 reduce_sum.113
  201.7 0.1 fusion.25
  201.8 0.2 multiply_reduce_fusion.1
  202.0 0.1 multiply_convert_fusion.2
  202.1 8.1 %all_to_all.27 = bf16[8,16,256]{2,1,0:T(8,128)(2,1)S(1)} all-to-all(bf16[8,16,256]{2,1,0:T(8,128)(2,1)S(1)} %bitcast.61), channel_id=1, replica_groups=mesh['grp'=2,'fs'=32,'tp'=8] {'tp'}, dimensions={0} | all-to-all | bytes 131072 | tf_op jit(solution)/shard_map/all_to_all | solution.py:41
  210.3 0.6 copy.44
  (17 shorter events, 0.2 us)
Async XLA Ops:
  6.5 110.1 %copy-start = (bf16[31,128]{1,0:T(8,128)(2,1)S(1)}, bf16[31,128]{1,0:T(8,128)(2,1)}, u32[]{:S(2)}) copy-start(bf16[31,128]{1,0:T(8,128)(2,1)} %param.16) | copy-start | bytes 23812
  6.6 99.2 %copy-start.1 = (bf16[1,128,2048]{2,1,0:T(8,128)(2,1)S(1)}, bf16[1,128,2048]{2,1,0:T(8,128)(2,1)}, u32[]{:S(2)}) copy-start(bf16[1,128,2048]{2,1,0:T(8,128)(2,1)} %param.12) | copy-start | bytes 1572868
  6.6 99.8 %copy-start.2 = (f32[2048]{0:T(1024)S(1)}, f32[2048]{0:T(1024)}, u32[]{:S(2)}) copy-start(f32[2048]{0:T(1024)} %param.13) | copy-start | bytes 24580
  6.6 166.8 %all-gather.3.cloned.1.call-start = ((), (), s32[]{:S(2)}) async-start(), calls=%async_computation.4 | async-start | bytes 4325376 | tf_op jit(solution)/shard_map/all_gather | solution.py:21
  98.9 16.6 %collective-permute-start = (bf16[3072,128]{1,0:T(8,128)(2,1)S(1)}, bf16[3072,128]{1,0:T(8,128)(2,1)S(1)}, u32[]{:S(2)}, u32[]{:S(2)}) collective-permute-start(bf16[3072,128]{1,0:T(8,128)(2,1)S(1)} %all_gather.9), channel_id=1, source_target_pairs={{0,256},{256,0},{1,257},{257,1},{2,258},{258,2},{3,259},{259,3},{4... | collective-permute-start | bytes 2359304 | tf_op jit(solution)/shard_map/ppermute | solution.py:91
  115.9 2.0 copy-start.4
  116.3 22.4 %copy-start.5 = (f32[128]{0:T(128)S(1)}, f32[128]{0:T(128)}, u32[]{:S(2)}) copy-start(f32[128]{0:T(128)} %param.18) | copy-start | bytes 1540
  116.3 22.4 %copy-start.6 = (f32[128]{0:T(128)S(1)}, f32[128]{0:T(128)}, u32[]{:S(2)}) copy-start(f32[128]{0:T(128)} %param.17) | copy-start | bytes 1540
  117.9 34.1 %copy-start.3 = (f32[2048]{0:T(1024)S(1)}, f32[2048]{0:T(1024)}, u32[]{:S(2)}) copy-start(f32[2048]{0:T(1024)} %param.20) | copy-start | bytes 24580
  152.1 5.7 %collective-permute-start.1 = (bf16[16,2048]{1,0:T(8,128)(2,1)S(1)}, bf16[16,2048]{1,0:T(8,128)(2,1)S(1)}, u32[]{:S(2)}, u32[]{:S(2)}) collective-permute-start(bf16[16,2048]{1,0:T(8,128)(2,1)S(1)} %multiply_convert_fusion.3), channel_id=1, source_target_pairs={{0,256},{256,0},{1,257},{257,1},{2,258},{258,2},{3,259},{259,3},{4... | collective-permute-start | bytes 196616 | tf_op jit(solution)/shard_map/ppermute | solution.py:140
  173.4 2.8 %copy-start.7 = (bf16[2048,1024]{1,0:T(8,128)(2,1)S(1)}, bf16[2048,1024]{1,0:T(8,128)(2,1)}, u32[]{:S(2)}) copy-start(bf16[2048,1024]{1,0:T(8,128)(2,1)} %all-gather.3.cloned.1.call-done) | copy-start | bytes 12582916
Sparse Core Ops, SparseCore 0:
  9.4 148.0 all-gather.2
where the time goes:
time: 218 us
  blocking collectives  170 us (78%)
  between operations  13.7 us (6%)
  waiting for transfers between devices  11.2 us (5%)
  starting transfers between devices  10.5 us (5%)
  matrix products  5.42 us (2%)
  other arithmetic  4.64 us (2%)
    all_gather x1, blocking collectives, gather_fs(): return lax.all_gather(x, 'fs', axis=0, tiled=True)  89.2 us
    all_to_all x3, blocking collectives, swap_blocks(): return lax.all_to_all(x, 'tp', 0, 0, tiled=True)  41.2 us
    all_to_all x1, blocking collectives, shards(): lax.all_to_all(fed_terms.reshape(sharing * tp_count, own_tokens, model_wi...  24.6 us
    all_gather x1, blocking collectives, shards(): lax.all_gather(to_half(pair_settled, feature_scale), 'tp', axis=0, tiled=...  15.3 us
    ppermute x1, waiting for transfers between devices, shards(): theirs = lax.ppermute(mine, 'grp', partner)  9.12 us
    ppermute x1, starting transfers between devices, shards(): theirs = lax.ppermute(mine, 'grp', partner)  6.85 us
  transfers between devices with their start and end apart: 3, of which 2 were waited for; matrix products, arithmetic and copies ran while one was open for 3% of the time, Pallas kernels for 0%

commit v1 on v0

--- a/solution.py
+++ b/solution.py
@@ -7,6 +7,19 @@
 norm_epsilon = 1e-05
 residual_scale = 2.0**0.25
 feature_scale = 2.0**7
+
+
+def collect(shard, axis, dim):
+    ways = lax.axis_size(axis)
+    up = [(d, (d + 1) % ways) for d in range(ways)]
+    down = [(d, (d - 1) % ways) for d in range(ways)]
+    earlier, later = ([shard], [shard])
+    for _ in range(ways // 2):
+        earlier.append(lax.ppermute(earlier[-1], axis, up))
+    for _ in range((ways - 1) // 2):
+        later.append(lax.ppermute(later[-1], axis, down))
+    line = jnp.concatenate([*earlier[::-1], *later[1:]], axis=dim)
+    return jnp.roll(line, (lax.axis_index(axis) - ways // 2) * shard.shape[dim], axis=dim)
 
 
 def to_half(x, scale):
@@ -142,8 +155,7 @@
     else:
         pair_settled = settled_own[None]
     settled = from_half(
-        lax.all_gather(to_half(pair_settled, feature_scale), "tp", axis=0, tiled=True),
-        feature_scale,
+        collect(to_half(pair_settled, feature_scale), "tp", 0), feature_scale
     ).reshape(sharing * token_count, model_width)
     hidden = jnp.square(
         jax.nn.relu(jnp.dot(settled, up_whole, preferred_element_type=jnp.float32))

time: 218 us -> 278 us (1.28)
  waiting for transfers between devices: 11.2 us -> 59.7 us
  starting transfers between devices: 10.5 us -> 20.8 us
    all_gather x1, waiting for transfers between devices: 0.02 us -> 43.5 us  [gather_fs(): return lax.all_gather(x, 'fs', axis=0, tiled=True)]
    all_to_all x1, blocking collectives: 24.6 us -> 40.2 us  [shards(): lax.all_to_all(fed_terms.reshape(sharing * tp_count, own_tokens, model_wi...]
    all_gather x1 -> x0, blocking collectives: 15.3 us -> none  [shards(): lax.all_gather(to_half(pair_settled, feature_scale), 'tp', axis=0, tiled=...]
    ppermute x0 -> x7, starting transfers between devices: none -> 13.5 us  [the longest x4 7.98 us: collect(): earlier.append(lax.ppermute(earlier[-1], axis, up))]
    ppermute x0 -> x7, waiting for transfers between devices: none -> 6.78 us  [the longest x4 4.55 us: collect(): earlier.append(lax.ppermute(earlier[-1], axis, up))]
    all_to_all x3, blocking collectives: 41.2 us -> 44.4 us  [swap_blocks(): return lax.all_to_all(x, 'tp', 0, 0, tiled=True)]
    ppermute x1, starting transfers between devices: 6.85 us -> 3.77 us  [shards(): theirs = lax.ppermute(mine, 'grp', partner)]
  transfers between devices with their start and end apart: 3 -> 10, of which waited for: 2 -> 10; matrix products, arithmetic and copies ran while one was open for 3% -> 2% of each run, Pallas kernels for 0% -> 0%
where the time goes in v1:
time: 278 us
  blocking collectives  171 us (62%)
  waiting for transfers between devices  59.7 us (21%)
  starting transfers between devices  20.8 us (7%)
  between operations  13.8 us (5%)
  matrix products  5.4 us (2%)
  other arithmetic  4.67 us (2%)
    all_gather x1, blocking collectives, gather_fs(): return lax.all_gather(x, 'fs', axis=0, tiled=True)  86.5 us
    all_to_all x3, blocking collectives, swap_blocks(): return lax.all_to_all(x, 'tp', 0, 0, tiled=True)  44.4 us
    all_gather x1, waiting for transfers between devices, gather_fs(): return lax.all_gather(x, 'fs', axis=0, tiled=True)  43.5 us
    all_to_all x1, blocking collectives, shards(): lax.all_to_all(fed_terms.reshape(sharing * tp_count, own_tokens, model_wi...  40.2 us
    ppermute x4, starting transfers between devices, collect(): earlier.append(lax.ppermute(earlier[-1], axis, up))  7.98 us
    ppermute x1, waiting for transfers between devices, shards(): theirs = lax.ppermute(mine, 'grp', partner)  7.34 us
  transfers between devices with their start and end apart: 10, of which 10 were waited for; matrix products, arithmetic and copies ran while one was open for 2% of the time, Pallas kernels for 0%

profile of v1, /device:TPU:33, one launch (start us, length us, event | category | flops | bytes accessed | tf_op | source)
XLA Modules:
  0.0 277.9 jit_solution(8868673079567310223)
XLA Ops:
  6.5 0.0 copy-start
  6.6 0.0 all-gather.2.cloned.1.call-start
  6.6 0.8 fusion.37
  7.3 0.7 maximum_select_fusion
  8.1 86.5 %all_gather.6 = bf16[3072,128]{1,0:T(8,128)(2,1)S(1)} all-gather(bf16[96,128]{1,0:T(8,128)(2,1)S(1)} %maximum_select_fusion), channel_id=1, replica_groups=mesh['grp'=2,'fs'=32,'tp'=8] {'fs'}, dimensions={0}, use_global_device_ids=true | all-gather | bytes 811008 | tf_op jit(solution)/shard_map/all_gather | solution.py:34
  94.6 3.8 %collective-permute-start = (bf16[3072,128]{1,0:T(8,128)(2,1)S(1)}, bf16[3072,128]{1,0:T(8,128)(2,1)S(1)}, u32[]{:S(2)}, u32[]{:S(2)}) collective-permute-start(bf16[3072,128]{1,0:T(8,128)(2,1)S(1)} %all_gather.6), channel_id=1, source_target_pairs={{0,256},{256,0},{1,257},{257,1},{2,258},{258,2},{3,259},{259,3},{4... | collective-permute-start | bytes 2359304 | tf_op jit(solution)/shard_map/ppermute | solution.py:104
  98.4 1.0 slice_select_fusion
  99.3 0.7 pad_maximum_fusion.1
  100.0 0.1 all-gather.2.cloned.1.call-update
  100.0 0.0 copy-done.1
  100.0 0.2 convert_reduce_fusion
  100.2 0.3 fusion.20
  100.5 0.1 dynamic-slice
  100.6 0.0 copy-done.2
  100.6 0.1 fusion.23
  100.7 7.3 %collective-permute-done = bf16[3072,128]{1,0:T(8,128)(2,1)S(1)} collective-permute-done((bf16[3072,128]{1,0:T(8,128)(2,1)S(1)}, bf16[3072,128]{1,0:T(8,128)(2,1)S(1)}, u32[]{:S(2)}, u32[]{:S(2)}) %collective-permute-start) | collective-permute-done | bytes 786464 | tf_op jit(solution)/shard_map/ppermute | solution.py:104
  108.0 0.1 broadcast_select_fusion.1
  108.1 0.1 slice.69
  108.2 0.4 fusion.14
  108.6 0.1 slice.68
  108.6 0.0 copy-start.4
  108.7 0.4 fusion.16
  109.0 0.0 copy-start.5
  109.0 0.0 copy-start.6
  109.1 0.0 copy-done
  109.1 1.1 fusion.38
  110.2 0.1 multiply_reduce_fusion.3
  110.3 0.0 copy-start.3
  110.4 0.1 pad_maximum_fusion
  110.4 23.7 %all_to_all.24 = f32[8,1,512]{2,1,0:T(1,128)S(1)} all-to-all(f32[8,1,512]{2,1,0:T(1,128)S(1)} %broadcast_in_dim.5), channel_id=1, replica_groups=mesh['grp'=2,'fs'=32,'tp'=8] {'tp'}, dimensions={0} | all-to-all | bytes 32768 | tf_op jit(solution)/shard_map/all_to_all | solution.py:54
  134.2 0.4 convolution_convert_fusion.1
  134.6 12.6 %all_to_all.25 = bf16[8,16,2048]{2,1,0:T(8,128)(2,1)S(1)} all-to-all(bf16[8,16,2048]{2,1,0:T(8,128)(2,1)S(1)} %bitcast.53), channel_id=1, replica_groups=mesh['grp'=2,'fs'=32,'tp'=8] {'tp'}, dimensions={0} | all-to-all | bytes 1048576 | tf_op jit(solution)/shard_map/all_to_all | solution.py:54
  147.2 0.1 reduce_sum.110
  147.2 0.1 fusion.24
  147.4 0.2 multiply_reduce_fusion.2
  147.6 0.1 multiply_convert_fusion.3
  147.7 3.6 %collective-permute-start.1 = (bf16[16,2048]{1,0:T(8,128)(2,1)S(1)}, bf16[16,2048]{1,0:T(8,128)(2,1)S(1)}, u32[]{:S(2)}, u32[]{:S(2)}) collective-permute-start(bf16[16,2048]{1,0:T(8,128)(2,1)S(1)} %multiply_convert_fusion.3), channel_id=1, source_target_pairs={{0,256},{256,0},{1,257},{257,1},{2,258},{258,2},{3,259},{259,3},{4... | collective-permute-start | bytes 196616 | tf_op jit(solution)/shard_map/ppermute | solution.py:153
  151.3 2.0 collective-permute-done.1
  153.4 1.8 collective-permute-start.2
  155.2 1.9 collective-permute-done.2
  157.1 2.4 collective-permute-start.3
  159.6 1.0 collective-permute-start.6
  160.6 0.9 collective-permute-done.3
  161.5 2.4 collective-permute-start.4
  164.0 0.4 collective-permute-done.6
  164.4 1.8 collective-permute-start.7
  166.2 0.8 collective-permute-done.4
  167.0 1.3 collective-permute-start.5
  168.4 0.8 collective-permute-done.7
  169.2 2.6 collective-permute-start.8
  171.8 0.8 collective-permute-done.5
  172.9 1.0 collective-permute-done.8
  174.2 0.2 multiply_convert_fusion
  174.4 43.5 %all-gather.2.cloned.1.call-done = bf16[2048,1024]{1,0:T(8,128)(2,1)} async-done(((bf16[64,1024]{1,0:T(8,128)(2,1)}), bf16[2048,1024]{1,0:T(8,128)(2,1)}) %all-gather.2.cloned.1.call-update) | async-done | bytes 4194320 | tf_op jit(solution)/shard_map/all_gather | solution.py:34
  217.9 2.4 fusion.9
  220.4 0.4 copy-done.7
  220.8 0.8 convolution_convert_fusion
  221.5 40.2 %all_to_all.26 = bf16[16,16,2048]{2,1,0:T(8,128)(2,1)S(1)} all-to-all(bf16[16,16,2048]{2,1,0:T(8,128)(2,1)S(1)} %bitcast.55), channel_id=1, replica_groups={{0,256,1,257,2,258,3,259,4,260,5,261,6,262,7,263},{8,264,9,265,10,266,1..., dimensions={0} | all-to-all | bytes 2097152 | tf_op jit(solution)/shard_map/all_to_all | solution.py:166
  261.7 0.1 reduce_sum.113
  261.8 0.1 fusion.25
  262.0 0.2 multiply_reduce_fusion.1
  262.2 0.1 multiply_convert_fusion.2
  262.3 8.1 %all_to_all.27 = bf16[8,16,256]{2,1,0:T(8,128)(2,1)S(1)} all-to-all(bf16[8,16,256]{2,1,0:T(8,128)(2,1)S(1)} %bitcast.61), channel_id=1, replica_groups=mesh['grp'=2,'fs'=32,'tp'=8] {'tp'}, dimensions={0} | all-to-all | bytes 131072 | tf_op jit(solution)/shard_map/all_to_all | solution.py:54
  270.4 0.6 copy.53
  (40 shorter events, 0.6 us)
Async XLA Ops:
  6.5 102.6 %copy-start = (bf16[31,128]{1,0:T(8,128)(2,1)S(1)}, bf16[31,128]{1,0:T(8,128)(2,1)}, u32[]{:S(2)}) copy-start(bf16[31,128]{1,0:T(8,128)(2,1)} %param.16) | copy-start | bytes 23812
  6.6 93.5 %copy-start.1 = (bf16[1,128,2048]{2,1,0:T(8,128)(2,1)S(1)}, bf16[1,128,2048]{2,1,0:T(8,128)(2,1)}, u32[]{:S(2)}) copy-start(bf16[1,128,2048]{2,1,0:T(8,128)(2,1)} %param.12) | copy-start | bytes 1572868
  6.6 94.0 %copy-start.2 = (f32[2048]{0:T(1024)S(1)}, f32[2048]{0:T(1024)}, u32[]{:S(2)}) copy-start(f32[2048]{0:T(1024)} %param.13) | copy-start | bytes 24580
  6.6 211.4 %all-gather.2.cloned.1.call-start = ((), (), s32[]{:S(2)}) async-start(), calls=%async_computation.4 | async-start | bytes 4325376 | tf_op jit(solution)/shard_map/all_gather | solution.py:34
  94.6 13.4 %collective-permute-start = (bf16[3072,128]{1,0:T(8,128)(2,1)S(1)}, bf16[3072,128]{1,0:T(8,128)(2,1)S(1)}, u32[]{:S(2)}, u32[]{:S(2)}) collective-permute-start(bf16[3072,128]{1,0:T(8,128)(2,1)S(1)} %all_gather.6), channel_id=1, source_target_pairs={{0,256},{256,0},{1,257},{257,1},{2,258},{258,2},{3,259},{259,3},{4... | collective-permute-start | bytes 2359304 | tf_op jit(solution)/shard_map/ppermute | solution.py:104
  108.6 1.7 copy-start.4
  109.0 25.2 %copy-start.5 = (f32[128]{0:T(128)S(1)}, f32[128]{0:T(128)}, u32[]{:S(2)}) copy-start(f32[128]{0:T(128)} %param.18) | copy-start | bytes 1540
  109.0 25.2 %copy-start.6 = (f32[128]{0:T(128)S(1)}, f32[128]{0:T(128)}, u32[]{:S(2)}) copy-start(f32[128]{0:T(128)} %param.17) | copy-start | bytes 1540
  110.3 37.3 %copy-start.3 = (f32[2048]{0:T(1024)S(1)}, f32[2048]{0:T(1024)}, u32[]{:S(2)}) copy-start(f32[2048]{0:T(1024)} %param.20) | copy-start | bytes 24580
  147.7 5.7 %collective-permute-start.1 = (bf16[16,2048]{1,0:T(8,128)(2,1)S(1)}, bf16[16,2048]{1,0:T(8,128)(2,1)S(1)}, u32[]{:S(2)}, u32[]{:S(2)}) collective-permute-start(bf16[16,2048]{1,0:T(8,128)(2,1)S(1)} %multiply_convert_fusion.3), channel_id=1, source_target_pairs={{0,256},{256,0},{1,257},{257,1},{2,258},{258,2},{3,259},{259,3},{4... | collective-permute-start | bytes 196616 | tf_op jit(solution)/shard_map/ppermute | solution.py:153
  153.4 3.7 %collective-permute-start.2 = (f16[2,16,2048]{2,1,0:T(8,128)(2,1)S(1)}, f16[2,16,2048]{2,1,0:T(8,128)(2,1)S(1)}, u32[]{:S(2)}, u32[]{:S(2)}) collective-permute-start(f16[2,16,2048]{2,1,0:T(8,128)(2,1)S(1)} %multiply_convert_fusion.1), channel_id=1, source_target_pairs={{0,1},{1,2},{2,3},{3,4},{4,5},{5,6},{6,7},{7,0},{8,9},{9,10},{10,1... | collective-permute-start | bytes 393224 | tf_op jit(solution)/shard_map/ppermute | solution.py:18
  157.1 4.4 %collective-permute-start.3 = (f16[2,16,2048]{2,1,0:T(8,128)(2,1)S(1)}, f16[2,16,2048]{2,1,0:T(8,128)(2,1)S(1)}, u32[]{:S(2)}, u32[]{:S(2)}) collective-permute-start(f16[2,16,2048]{2,1,0:T(8,128)(2,1)S(1)} %collective-permute-done.2), channel_id=1, source_target_pairs={{0,1},{1,2},{2,3},{3,4},{4,5},{5,6},{6,7},{7,0},{8,9},{9,10},{10,1... | collective-permute-start | bytes 393224 | tf_op jit(solution)/shard_map/ppermute | solution.py:18
  159.6 4.8 %collective-permute-start.6 = (f16[2,16,2048]{2,1,0:T(8,128)(2,1)S(1)}, f16[2,16,2048]{2,1,0:T(8,128)(2,1)S(1)}, u32[]{:S(2)}, u32[]{:S(2)}) collective-permute-start(f16[2,16,2048]{2,1,0:T(8,128)(2,1)S(1)} %multiply_convert_fusion.1), channel_id=1, source_target_pairs={{0,7},{1,0},{2,1},{3,2},{4,3},{5,4},{6,5},{7,6},{8,15},{9,8},{10,9... | collective-permute-start | bytes 393224 | tf_op jit(solution)/shard_map/ppermute | solution.py:20
  161.5 5.5 %collective-permute-start.4 = (f16[2,16,2048]{2,1,0:T(8,128)(2,1)S(1)}, f16[2,16,2048]{2,1,0:T(8,128)(2,1)S(1)}, u32[]{:S(2)}, u32[]{:S(2)}) collective-permute-start(f16[2,16,2048]{2,1,0:T(8,128)(2,1)S(1)} %collective-permute-done.3), channel_id=1, source_target_pairs={{0,1},{1,2},{2,3},{3,4},{4,5},{5,6},{6,7},{7,0},{8,9},{9,10},{10,1... | collective-permute-start | bytes 393224 | tf_op jit(solution)/shard_map/ppermute | solution.py:18
  164.4 4.8 %collective-permute-start.7 = (f16[2,16,2048]{2,1,0:T(8,128)(2,1)S(1)}, f16[2,16,2048]{2,1,0:T(8,128)(2,1)S(1)}, u32[]{:S(2)}, u32[]{:S(2)}) collective-permute-start(f16[2,16,2048]{2,1,0:T(8,128)(2,1)S(1)} %collective-permute-done.6), channel_id=1, source_target_pairs={{0,7},{1,0},{2,1},{3,2},{4,3},{5,4},{6,5},{7,6},{8,15},{9,8},{10,9... | collective-permute-start | bytes 393224 | tf_op jit(solution)/shard_map/ppermute | solution.py:20
  167.0 5.6 %collective-permute-start.5 = (f16[2,16,2048]{2,1,0:T(8,128)(2,1)S(1)}, f16[2,16,2048]{2,1,0:T(8,128)(2,1)S(1)}, u32[]{:S(2)}, u32[]{:S(2)}) collective-permute-start(f16[2,16,2048]{2,1,0:T(8,128)(2,1)S(1)} %collective-permute-done.4), channel_id=1, source_target_pairs={{0,1},{1,2},{2,3},{3,4},{4,5},{5,6},{6,7},{7,0},{8,9},{9,10},{10,1... | collective-permute-start | bytes 393224 | tf_op jit(solution)/shard_map/ppermute | solution.py:18
  169.2 4.7 %collective-permute-start.8 = (f16[2,16,2048]{2,1,0:T(8,128)(2,1)S(1)}, f16[2,16,2048]{2,1,0:T(8,128)(2,1)S(1)}, u32[]{:S(2)}, u32[]{:S(2)}) collective-permute-start(f16[2,16,2048]{2,1,0:T(8,128)(2,1)S(1)} %collective-permute-done.7), channel_id=1, source_target_pairs={{0,7},{1,0},{2,1},{3,2},{4,3},{5,4},{6,5},{7,6},{8,15},{9,8},{10,9... | collective-permute-start | bytes 393224 | tf_op jit(solution)/shard_map/ppermute | solution.py:20
  217.9 2.8 %copy-start.7 = (bf16[2048,1024]{1,0:T(8,128)(2,1)S(1)}, bf16[2048,1024]{1,0:T(8,128)(2,1)}, u32[]{:S(2)}) copy-start(bf16[2048,1024]{1,0:T(8,128)(2,1)} %all-gather.2.cloned.1.call-done) | copy-start | bytes 12582916
Sparse Core Ops, SparseCore 0:
  100.1 117.7 all-gather.1
